TPU v7x, 128 devices: a whole 4x4x4 slice. The times are simulated.
128 devices in a mesh: sp: 16 (over z, x), tp: 8 (over y, core).
Axes of the slice: x: 4, y: 4, z: 4, core: 2. Of those that a mesh axis runs over, the one named last changes fastest.
Arguments:
- tokens_in: bfloat16 [12288, 2048], P(('sp', 'tp')), may hold values from -300 to 300
- norm_gain: float32 [2048], replicated, may hold values from 0.1 to 1.9
- query_weight: bfloat16 [2048, 1024], P('sp', 'tp'), may hold values from -64 to 64
- key_weight: bfloat16 [2048, 512], P('sp', 'tp'), may hold values from -1 to 1
- value_weight: bfloat16 [2048, 512], P('sp', 'tp'), may hold values from -0.125 to 0.125
- pool_weight: bfloat16 [2048, 1024], P('sp', 'tp'), may hold values from -0.125 to 0.125
- sink_logit: float32 [16], P('tp'), may hold values from 1 to 5
- pool_gain: float32 [1024], P('tp'), may hold values from 0.1 to 1.9
- attention_out_weight: bfloat16 [1024, 2048], P('tp', 'sp'), may hold values from -0.125 to 0.125
- pool_out_weight: bfloat16 [1024, 2048], P('tp', 'sp'), may hold values from -0.1875 to 0.1875
Outputs:
- mixed_out: bfloat16 [12288, 2048], P(('sp', 'tp'))
All inputs are finite; a program needn't handle non-finite values.
Results may differ from a plain program's by a relative error of at most 0.014.
Values may be sent and summed in bfloat16 or wider, within the bound.
A program may use at most 64 MiB of HBM per device.

v0:
```python
import jax
import jax.numpy as jnp
from jax import lax
from jax.sharding import PartitionSpec as P

HEAD_DIM = 64
POOL_CH = 256
POOL_GROUPS = 4
WINDOW = 128
EPS = 1e-06
SHORT_REACHES = (8, 32)


def sent_together(arrays, axis, dim, along):
    ends, at = ([], 0)
    for a in arrays[:-1]:
        at += a.shape[along]
        ends.append(at)
    both = jnp.concatenate(arrays, axis=along)
    return tuple(jnp.split(lax.all_gather(both, axis, axis=dim, tiled=True), ends, axis=along))


def passed_along(block, axis, distance):
    devices = range(lax.axis_size(axis))
    route = [(i - distance, i) for i in devices if i - distance in devices]
    return lax.ppermute(block, axis, route)


def from_everyone(x, axis):
    copies = jnp.broadcast_to(x, (lax.axis_size(axis), *x.shape))
    return lax.all_to_all(copies, axis, split_axis=0, concat_axis=0, tiled=True)


def in_order(parts, dim):
    parts = jnp.moveaxis(parts, 0, dim)
    shape = parts.shape
    return parts.reshape(*shape[:dim], shape[dim] * shape[dim + 1], *shape[dim + 2 :])


def gathered_copies(x, axis, dim):
    parts = from_everyone(x, axis)
    return in_order(parts, dim)


def local(
    tokens_in,
    norm_gain,
    query_weight,
    key_weight,
    value_weight,
    pool_weight,
    sink_logit,
    pool_gain,
    attention_out_weight,
    pool_out_weight,
):
    widened = tokens_in.astype(jnp.float32)
    inverse = lax.rsqrt(jnp.mean(widened * widened, axis=1, keepdims=True) + EPS)
    normed = (widened * inverse * norm_gain).astype(jnp.bfloat16)
    all_rows = lax.all_gather(normed, "tp", axis=0, tiled=True)
    pieces = sent_together((query_weight, key_weight, value_weight, pool_weight), "sp", 0, 1)
    projected = tuple(
        (
            jnp.dot(all_rows, weight_piece, preferred_element_type=jnp.float32)
            for weight_piece in pieces
        )
    )
    query_rows, key_rows, value_rows, pool_rows = [
        projection.astype(jnp.bfloat16) for projection in projected
    ]
    seq_len = query_rows.shape[0]
    offset = lax.axis_index("sp") * seq_len
    halo_keys, halo_values, halo_pool = passed_along(
        (
            key_rows[seq_len - WINDOW :],
            value_rows[seq_len - WINDOW :],
            pool_rows[seq_len - WINDOW :],
        ),
        "sp",
        1,
    )
    kv_local = key_rows.shape[1] // HEAD_DIM
    heads_local = query_rows.shape[1] // HEAD_DIM
    group = heads_local // kv_local
    blocks = seq_len // WINDOW
    key_ext = jnp.concatenate([halo_keys, key_rows], axis=0).reshape(
        blocks + 1, WINDOW, kv_local, HEAD_DIM
    )
    value_ext = jnp.concatenate([halo_values, value_rows], axis=0).reshape(
        blocks + 1, WINDOW, kv_local, HEAD_DIM
    )
    key_pairs = jnp.concatenate([key_ext[:-1], key_ext[1:]], axis=1)
    value_pairs = jnp.concatenate([value_ext[:-1], value_ext[1:]], axis=1)
    query_blocks = query_rows.reshape(blocks, WINDOW, kv_local, group, HEAD_DIM)
    scores = jnp.einsum(
        "nqhgd,nkhd->nhgqk", query_blocks, key_pairs, preferred_element_type=jnp.float32
    ) * HEAD_DIM ** (-0.5)
    shape_mask = (blocks, WINDOW, 2 * WINDOW)
    q_index = lax.broadcasted_iota(jnp.int32, shape_mask, 1)
    k_index = lax.broadcasted_iota(jnp.int32, shape_mask, 2)
    block_index = lax.broadcasted_iota(jnp.int32, shape_mask, 0)
    distance = q_index + WINDOW - k_index
    key_position = offset + block_index * WINDOW + k_index - WINDOW
    allowed = (distance >= 0) & (distance < WINDOW) & (key_position >= 0)
    scores = jnp.where(allowed[:, None, None], scores, -jnp.inf)
    sinks = sink_logit.reshape(1, kv_local, group, 1, 1)
    peak = jnp.maximum(jnp.max(scores, axis=-1, keepdims=True), sinks)
    expo = jnp.exp(scores - peak)
    denom = jnp.sum(expo, axis=-1, keepdims=True) + jnp.exp(sinks - peak)
    probs = (expo / denom).astype(jnp.bfloat16)
    attended = jnp.einsum(
        "nhgqk,nkhd->nqhgd", probs, value_pairs, preferred_element_type=jnp.float32
    )
    attended = attended.astype(jnp.bfloat16).reshape(seq_len, heads_local * HEAD_DIM)
    pool_values = pool_rows.astype(jnp.float32)
    channels = pool_rows.shape[1]
    pool_ext = jnp.concatenate([halo_pool.astype(jnp.float32), pool_values], axis=0)
    running = jnp.concatenate(
        [jnp.zeros((1, channels), jnp.float32), jnp.cumsum(pool_ext, axis=0)], axis=0
    )
    group_id = lax.axis_index("tp") * channels // POOL_CH
    reach = jnp.where(
        group_id == 0, SHORT_REACHES[0], jnp.where(group_id == 1, SHORT_REACHES[1], WINDOW)
    ).astype(jnp.int32)
    upper = running[WINDOW + 1 :]
    lower = lax.dynamic_slice_in_dim(running, WINDOW + 1 - reach, seq_len, 0)
    position = offset + lax.broadcasted_iota(jnp.int32, (seq_len,), 0)
    counted = jnp.minimum(position + 1, reach).astype(jnp.float32)[:, None]
    windowed = (upper - lower) / counted
    own_sums = upper - running[WINDOW]
    device_total = own_sums[seq_len - 1]
    totals = gathered_copies(device_total[None, :], "sp", 0)
    earlier_rows = lax.broadcasted_iota(jnp.int32, (totals.shape[0], 1), 0) < lax.axis_index("sp")
    before = jnp.sum(jnp.where(earlier_rows, totals, 0.0), axis=0)
    cumulative = (before[None, :] + own_sums) / (position + 1).astype(jnp.float32)[:, None]
    pooled = jnp.where(group_id == POOL_GROUPS - 1, cumulative, windowed)
    pool_mixed = ((pooled - pool_values) * pool_gain).astype(jnp.bfloat16)
    out_attend, out_pool = sent_together((attention_out_weight, pool_out_weight), "sp", 1, 0)
    return lax.psum_scatter(
        (
            jnp.dot(attended, out_attend, preferred_element_type=jnp.float32)
            + jnp.dot(pool_mixed, out_pool, preferred_element_type=jnp.float32)
        ).astype(jnp.bfloat16),
        "tp",
        scatter_dimension=0,
        tiled=True,
    )


def solution(mesh):
    in_specs = (
        P(("sp", "tp"), None),
        P(),
        P("sp", "tp"),
        P("sp", "tp"),
        P("sp", "tp"),
        P("sp", "tp"),
        P("tp"),
        P("tp"),
        P("tp", "sp"),
        P("tp", "sp"),
    )
    out_specs = P(("sp", "tp"), None)
    return jax.shard_map(local, mesh=mesh, in_specs=in_specs, out_specs=out_specs, check_vma=False)
```

profile of v0, /device:TPU:0, one launch (start us, length us, event | category | flops | bytes accessed | tf_op | source)
XLA Modules:
  0.0 182.7 jit_solution(4462187103619193170)
XLA Ops:
  6.5 0.0 all-gather.6.cloned.1.call-start
  6.5 0.8 copy.33
  7.4 0.8 copy.34
  8.2 1.5 pad_maximum_fusion.3
  9.7 0.0 all-gather.6.cloned.1.call-update
  9.7 0.0 all-gather.4.cloned.1.call-start
  9.8 1.2 fusion.2
  11.0 1.9 %fusion.4 = bf16[96,2048]{1,0:T(8,128)(2,1)} fusion(bf16[96,2048]{1,0:T(8,128)(2,1)} %param.10, f32[2048]{0:T(1024)} %param.11, f32[96]{0:T(128)S(1)} %add_rsqrt_fusion), kind=kLoop, calls=%fused_computation.15 | loop fusion | flops 786432 | bytes 795008 | tf_op jit(solution)/shard_map/convert_element_type | solution.py:59
  12.9 0.0 all-gather.4.cloned.1.call-update
  12.9 0.0 all-gather.8.cloned.1.call-start
  13.0 0.0 copy-done.8
  13.0 0.0 copy-done.9
  13.0 0.6 pad_maximum_fusion.4
  13.6 0.0 all-gather.8.cloned.1.call-update
  13.8 1.0 fusion.8
  14.7 41.5 %all-gather.6.cloned.1.call-done = bf16[2048,384]{1,0:T(8,128)(2,1)} async-done(((bf16[128,384]{1,0:T(8,128)(2,1)}), bf16[2048,384]{1,0:T(8,128)(2,1)}) %all-gather.6.cloned.1.call-update) | async-done | bytes 1572880 | tf_op jit(solution)/shard_map/all_gather | solution.py:20
  56.2 28.7 %all-gather.4.cloned.1.call-done = bf16[768,2048]{1,0:T(8,128)(2,1)} async-done(((bf16[96,2048]{1,0:T(8,128)(2,1)}), bf16[768,2048]{1,0:T(8,128)(2,1)}) %all-gather.4.cloned.1.call-update) | async-done | bytes 3145744 | tf_op jit(solution)/shard_map/all_gather | solution.py:60
  84.9 3.2 %convolution_convert_fusion.3 = bf16[768,64]{0,1:T(8,128)(2,1)S(1)} fusion(bf16[768,2048]{1,0:T(8,128)(2,1)} %all-gather.4.cloned.1.call-done, bf16[2048,384]{1,0:T(8,128)(2,1)} %all-gather.6.cloned.1.call-done), kind=kOutput, calls=%fused_computation.9 | convolution fusion | flops 201375744 | bytes 3768320 | tf_op jit(solution)/shard_map/dot_general | solution.py:64
  88.1 0.6 slice.62
  88.7 0.0 copy-done.6
  88.8 0.1 slice.53
  88.9 0.0 copy-done
  88.9 2.2 %convolution_convert_fusion.4 = bf16[768,64]{0,1:T(8,128)(2,1)S(1)} fusion(bf16[768,2048]{1,0:T(8,128)(2,1)S(1)} %copy-done, bf16[2048,384]{1,0:T(8,128)(2,1)} %all-gather.6.cloned.1.call-done), kind=kOutput, calls=%fused_computation.10 | convolution fusion | flops 201375744 | bytes 3768320 | tf_op jit(solution)/shard_map/dot_general | solution.py:64
  91.1 0.6 slice.61
  91.8 0.1 slice.49
  91.9 4.0 %collective-permute-start.1 = (bf16[128,64]{0,1:T(8,128)(2,1)}, bf16[128,64]{0,1:T(8,128)(2,1)}, u32[]{:S(2)}, u32[]{:S(2)}) collective-permute-start(bf16[128,64]{0,1:T(8,128)(2,1)} %slice.62), channel_id=1, source_target_pairs={{0,8},{8,16},{16,24},{24,32},{32,40},{40,48},{48,56},{56,64},{64,7... | collective-permute-start | bytes 49160 | tf_op jit(solution)/shard_map/ppermute | solution.py:26
  95.9 0.6 copy.38
  96.5 3.4 %collective-permute-start = (bf16[128,64]{0,1:T(8,128)(2,1)}, bf16[128,64]{0,1:T(8,128)(2,1)}, u32[]{:S(2)}, u32[]{:S(2)}) collective-permute-start(bf16[128,64]{0,1:T(8,128)(2,1)} %slice.61), channel_id=1, source_target_pairs={{0,8},{8,16},{16,24},{24,32},{32,40},{40,48},{48,56},{56,64},{64,7... | collective-permute-start | bytes 49160 | tf_op jit(solution)/shard_map/ppermute | solution.py:26
  99.9 0.0 copy-done.4
  99.9 0.6 copy.36
  100.6 2.0 %fusion.45 = (f32[768,128]{1,0:T(8,128)S(1)}, bf16[768,128]{1,0:T(8,128)(2,1)S(1)}) fusion(bf16[768,2048]{1,0:T(8,128)(2,1)S(1)} %copy-done, bf16[2048,384]{1,0:T(8,128)(2,1)} %all-gather.6.cloned.1.call-done), kind=kOutput, calls=%fused_computation.79 | convolution fusion | flops 402849792 | bytes 4259840 | tf_op jit(solution)/shard_map/dot_general | solution.py:64
  102.6 0.7 copy-done.1
  103.2 0.6 slice.63
  103.8 3.1 %collective-permute-start.2 = (bf16[128,128]{1,0:T(8,128)(2,1)}, bf16[128,128]{1,0:T(8,128)(2,1)}, u32[]{:S(2)}, u32[]{:S(2)}) collective-permute-start(bf16[128,128]{1,0:T(8,128)(2,1)} %slice.63), channel_id=1, source_target_pairs={{0,8},{8,16},{16,24},{24,32},{32,40},{40,48},{48,56},{56,64},{64,7... | collective-permute-start | bytes 98312 | tf_op jit(solution)/shard_map/ppermute | solution.py:26
  106.9 2.7 %convolution_convert_fusion.1 = bf16[768,128]{1,0:T(8,128)(2,1)} fusion(bf16[768,2048]{1,0:T(8,128)(2,1)S(1)} %copy-done, bf16[2048,384]{1,0:T(8,128)(2,1)} %all-gather.6.cloned.1.call-done), kind=kOutput, calls=%fused_computation.6 | convolution fusion | flops 402751488 | bytes 3866624 | tf_op jit(solution)/shard_map/dot_general | solution.py:64
  109.6 1.1 reshape.121
  110.7 0.0 collective-permute-done.1
  110.8 0.9 pad_maximum_fusion.1
  111.7 0.0 copy-start.10
  111.7 0.1 slice.52
  111.8 1.5 fusion.44
  113.3 0.1 broadcast_maximum_fusion
  113.4 0.2 fusion
  113.7 0.1 exponential_add_fusion
  113.7 0.0 collective-permute-done
  113.8 0.7 pad_maximum_fusion.2
  114.5 0.1 slice.48
  114.7 0.4 fusion.1
  115.1 0.1 copy.42
  115.2 0.0 collective-permute-done.2
  115.2 0.8 convert_element_type.66
  116.0 0.3 fusion.17
  116.4 0.1 copy.44
  116.5 0.6 broadcast_in_dim.40
  117.1 6.1 %all-to-all-start = ((f32[16,1,128]{2,1,0:T(1,128)}), f32[16,1,128]{2,1,0:T(1,128)S(1)}, u32[]{:S(2)}, u32[]{:S(2)}) async-start(f32[16,1,128]{2,1,0:T(1,128)} %broadcast_in_dim.40), calls=%async_computation | async-start | bytes 16384 | tf_op jit(solution)/shard_map/all_to_all | solution.py:31
  123.3 0.0 reduce-scatter.2.cloned.1.call-start
  123.3 7.0 %all-gather.8.cloned.1.call-done = bf16[256,2048]{1,0:T(8,128)(2,1)} async-done(((bf16[256,128]{1,0:T(8,128)(2,1)}), bf16[256,2048]{1,0:T(8,128)(2,1)}) %all-gather.8.cloned.1.call-update) | async-done | bytes 1048592 | tf_op jit(solution)/shard_map/all_gather | solution.py:20
  130.3 4.8 %fusion.12 = f32[768,2048]{1,0:T(8,128)} fusion(bf16[256,2048]{1,0:T(8,128)(2,1)} %all-gather.8.cloned.1.call-done, bf16[16,8,6,128]{3,2,1,0:T(8,128)(2,1)S(1)} %bitcast.62), kind=kOutput, calls=%fused_computation.25 | convolution fusion | flops 402653184 | bytes 7012352 | tf_op jit(solution)/shard_map/dot_general | solution.py:141
  135.1 0.0 all-to-all-done
  135.1 0.1 select_reduce_fusion
  135.2 0.0 copy-done.2
  135.2 5.6 %add_convert_fusion = bf16[768,2048]{1,0:T(8,128)(2,1)} fusion(f32[768,2048]{1,0:T(8,128)} %fusion.12, bf16[256,2048]{1,0:T(8,128)(2,1)S(1)} %copy-done.3, s32[]{:T(128)S(6)} %select_n.38, f32[896,128]{1,0:T(8,128)S(1)} %bitcast.60, f32[768,128]{1,0:T(8,128)S(1)} %slice_subtract_fusion, f32[128]{0:T(128)S(1)} %copy-done.11, f32[768]{0:T(1024)S(1)} %get-tuple-element.9, ...), kind=kOutput, calls=%fused_computation | convolution fusion | flops 406683648 | bytes 11412485 | tf_op jit(solution)/shard_map/dot_general | solution.py:142
  140.8 0.0 reduce-scatter.2.cloned.1.call-update
  140.8 35.3 %reduce-scatter.2.cloned.1.call-done = bf16[96,2048]{1,0:T(8,128)(2,1)} async-done(((bf16[768,2048]{1,0:T(8,128)(2,1)}), bf16[96,2048]{1,0:T(8,128)(2,1)}) %reduce-scatter.2.cloned.1.call-update) | async-done | bytes 393232 | tf_op jit(solution)/shard_map/reduce_scatter | solution.py:139
  (30 shorter events, 0.2 us)
Async XLA Ops:
  6.5 6.4 %copy-start.8 = (bf16[128,128]{1,0:T(8,128)(2,1)S(1)}, bf16[128,128]{1,0:T(8,128)(2,1)}, u32[]{:S(2)}) copy-start(bf16[128,128]{1,0:T(8,128)(2,1)} %param.19) | copy-start | bytes 98308
  6.5 6.5 %copy-start.9 = (bf16[128,128]{1,0:T(8,128)(2,1)S(1)}, bf16[128,128]{1,0:T(8,128)(2,1)}, u32[]{:S(2)}) copy-start(bf16[128,128]{1,0:T(8,128)(2,1)} %param.18) | copy-start | bytes 98308
  6.5 49.7 %all-gather.6.cloned.1.call-start = ((), (), s32[]{:S(2)}) async-start(), calls=%async_computation.3 | async-start | bytes 1671168 | tf_op jit(solution)/shard_map/all_gather | solution.py:20
  9.7 75.1 %all-gather.4.cloned.1.call-start = ((), (), s32[]{:S(2)}) async-start(), calls=%async_computation.2 | async-start | bytes 3538944 | tf_op jit(solution)/shard_map/all_gather | solution.py:60
  12.9 117.4 %all-gather.8.cloned.1.call-start = ((), (), s32[]{:S(2)}) async-start(), calls=%async_computation.4 | async-start | bytes 1114112 | tf_op jit(solution)/shard_map/all_gather | solution.py:20
  84.9 4.0 %copy-start = (bf16[768,2048]{1,0:T(8,128)(2,1)S(1)}, bf16[768,2048]{1,0:T(8,128)(2,1)}, u32[]{:S(2)}) copy-start(bf16[768,2048]{1,0:T(8,128)(2,1)} %all-gather.4.cloned.1.call-done) | copy-start | bytes 9437188
  88.1 0.7 copy-start.6
  91.1 8.8 %copy-start.4 = (bf16[768,64]{0,1:T(8,128)(2,1)}, bf16[768,64]{0,1:T(8,128)(2,1)S(1)}, u32[]{:S(2)}) copy-start(bf16[768,64]{0,1:T(8,128)(2,1)S(1)} %convolution_convert_fusion.4) | copy-start | bytes 294916
  91.9 18.8 %collective-permute-start.1 = (bf16[128,64]{0,1:T(8,128)(2,1)}, bf16[128,64]{0,1:T(8,128)(2,1)}, u32[]{:S(2)}, u32[]{:S(2)}) collective-permute-start(bf16[128,64]{0,1:T(8,128)(2,1)} %slice.62), channel_id=1, source_target_pairs={{0,8},{8,16},{16,24},{24,32},{32,40},{40,48},{48,56},{56,64},{64,7... | collective-permute-start | bytes 49160 | tf_op jit(solution)/shard_map/ppermute | solution.py:26
  96.5 17.2 %collective-permute-start = (bf16[128,64]{0,1:T(8,128)(2,1)}, bf16[128,64]{0,1:T(8,128)(2,1)}, u32[]{:S(2)}, u32[]{:S(2)}) collective-permute-start(bf16[128,64]{0,1:T(8,128)(2,1)} %slice.61), channel_id=1, source_target_pairs={{0,8},{8,16},{16,24},{24,32},{32,40},{40,48},{48,56},{56,64},{64,7... | collective-permute-start | bytes 49160 | tf_op jit(solution)/shard_map/ppermute | solution.py:26
  102.6 0.7 copy-start.1
  103.8 11.4 %collective-permute-start.2 = (bf16[128,128]{1,0:T(8,128)(2,1)}, bf16[128,128]{1,0:T(8,128)(2,1)}, u32[]{:S(2)}, u32[]{:S(2)}) collective-permute-start(bf16[128,128]{1,0:T(8,128)(2,1)} %slice.63), channel_id=1, source_target_pairs={{0,8},{8,16},{16,24},{24,32},{32,40},{40,48},{48,56},{56,64},{64,7... | collective-permute-start | bytes 98312 | tf_op jit(solution)/shard_map/ppermute | solution.py:26
  111.7 1.7 copy-start.10
  111.8 1.9 %copy-start.5 = (bf16[768,64]{0,1:T(8,128)(2,1)S(1)}, bf16[768,64]{0,1:T(8,128)(2,1)}, u32[]{:S(2)}) copy-start(bf16[768,64]{0,1:T(8,128)(2,1)} %copy-done.4) | copy-start | bytes 294916
  113.3 1.3 copy-start.7
  117.1 18.0 %all-to-all-start = ((f32[16,1,128]{2,1,0:T(1,128)}), f32[16,1,128]{2,1,0:T(1,128)S(1)}, u32[]{:S(2)}, u32[]{:S(2)}) async-start(f32[16,1,128]{2,1,0:T(1,128)} %broadcast_in_dim.40), calls=%async_computation | async-start | bytes 16384 | tf_op jit(solution)/shard_map/all_to_all | solution.py:31
  123.3 52.8 %reduce-scatter.2.cloned.1.call-start = ((), (), s32[]{:S(2)}) async-start(), calls=%async_computation.5 | async-start | bytes 3538944 | tf_op jit(solution)/shard_map/reduce_scatter | solution.py:139
  130.3 4.9 %copy-start.2 = (bf16[768,128]{1,0:T(8,128)(2,1)S(1)}, bf16[768,128]{1,0:T(8,128)(2,1)}, u32[]{:S(2)}) copy-start(bf16[768,128]{1,0:T(8,128)(2,1)} %copy-done.1) | copy-start | bytes 589828
  130.3 4.9 %copy-start.3 = (bf16[256,2048]{1,0:T(8,128)(2,1)S(1)}, bf16[256,2048]{1,0:T(8,128)(2,1)}, u32[]{:S(2)}) copy-start(bf16[256,2048]{1,0:T(8,128)(2,1)} %all-gather.8.cloned.1.call-done) | copy-start | bytes 3145732
  130.3 4.9 %copy-start.11 = (f32[128]{0:T(128)S(1)}, f32[128]{0:T(128)}, u32[]{:S(2)}) copy-start(f32[128]{0:T(128)} %param.17) | copy-start | bytes 1540
Sparse Core Ops, SparseCore 0:
  9.9 46.2 all-gather.5
  57.9 26.9 all-gather.3
  87.0 43.2 all-gather.7
  141.0 35.1 reduce-scatter.1
where the time goes:
time: 183 us
  waiting for transfers between devices  112 us (61%)
  matrix products  22.4 us (12%)
  starting transfers between devices  16.7 us (9%)
  between operations  13.5 us (7%)
  other arithmetic  9.51 us (5%)
  local copies, waits for them, and re-layouts  8.08 us (4%)
    all_gather x2, waiting for transfers between devices, sent_together(): lax.all_gather(both, axis, axis=dim, tiled=True)  48.4 us
    reduce_scatter x1, waiting for transfers between devices, local(): lax.psum_scatter((jnp.dot(attended, out_attend, preferred_element_type=jn...  35.3 us
    all_gather x1, waiting for transfers between devices, local(): all_rows = lax.all_gather(normed, 'tp', axis=0, tiled=True)  28.7 us
    ppermute x3, starting transfers between devices, passed_along(): return lax.ppermute(block, axis, route)  10.4 us
    dot_general x4, matrix products, local(): jnp.dot(all_rows, weight_piece, preferred_element_type=jnp.float32)  10.1 us
    all_to_all x1, starting transfers between devices, from_everyone(): return lax.all_to_all(copies, axis, split_axis=0, concat_axis=0, tiled=True)  6.14 us
    dot_general x1, matrix products, local(): jnp.dot(pool_mixed, out_pool, preferred_element_type=jnp.float32)  5.6 us
    dot_general x1, matrix products, local(): jnp.dot(attended, out_attend, preferred_element_type=jnp.float32)  4.8 us
  transfers between devices with their start and end apart: 8, of which 4 were waited for; matrix products, arithmetic and copies ran while one was open for 17% of the time, Pallas kernels for 0%

commit v1 on v0

--- a/solution.py
+++ b/solution.py
@@ -57,7 +57,9 @@
     widened = tokens_in.astype(jnp.float32)
     inverse = lax.rsqrt(jnp.mean(widened * widened, axis=1, keepdims=True) + EPS)
     normed = (widened * inverse * norm_gain).astype(jnp.bfloat16)
-    all_rows = lax.all_gather(normed, "tp", axis=0, tiled=True)
+    all_rows = jnp.concatenate(
+        lax.all_to_all(jnp.stack([normed] * lax.axis_size("tp")), "tp", 0, 0), axis=0
+    )
     pieces = sent_together((query_weight, key_weight, value_weight, pool_weight), "sp", 0, 1)
     projected = tuple(
         (

time: 183 us -> 154 us (0.84)
  waiting for transfers between devices: 112 us -> 77.2 us
  starting transfers between devices: 16.7 us -> 22.5 us
  local copies, waits for them, and re-layouts: 8.08 us -> 10.1 us
    all_gather x2, waiting for transfers between devices: 48.4 us -> 5.16 us  [sent_together(): lax.all_gather(both, axis, axis=dim, tiled=True)]
    all_to_all x0 -> x1, waiting for transfers between devices: none -> 36.6 us  [local(): lax.all_to_all(jnp.stack([normed] * lax.axis_size('tp')), 'tp', 0, 0)]
    all_gather x1 -> x0, waiting for transfers between devices: 28.7 us -> none  [local(): all_rows = lax.all_gather(normed, 'tp', axis=0, tiled=True)]
    all_to_all x0 -> x1, starting transfers between devices: none -> 4.71 us  [local(): lax.all_to_all(jnp.stack([normed] * lax.axis_size('tp')), 'tp', 0, 0)]
    another operation x3 -> x4, local copies, waits for them, and re-layouts: 1.2 us -> 3.23 us  [the longest x1 2.03 us: local(): jnp.stack([normed] * lax.axis_size('tp'))]
  transfers between devices with their start and end apart: 8 -> 8, of which waited for: 4 -> 3; matrix products, arithmetic and copies ran while one was open for 17% -> 20% of each run, Pallas kernels for 0% -> 0%
where the time goes in v1:
time: 154 us; the launch traced here: 153 us
  waiting for transfers between devices  77.2 us (50%)
  starting transfers between devices  22.5 us (15%)
  matrix products  21.3 us (14%)
  between operations  13.4 us (9%)
  local copies, waits for them, and re-layouts  10.1 us (7%)
  other arithmetic  8.76 us (6%)
    all_to_all x1, waiting for transfers between devices, local(): lax.all_to_all(jnp.stack([normed] * lax.axis_size('tp')), 'tp', 0, 0)  36.6 us
    reduce_scatter x1, waiting for transfers between devices, local(): lax.psum_scatter((jnp.dot(attended, out_attend, preferred_element_type=jn...  35.3 us
    ppermute x3, starting transfers between devices, passed_along(): return lax.ppermute(block, axis, route)  10.5 us
    dot_general x4, matrix products, local(): jnp.dot(all_rows, weight_piece, preferred_element_type=jnp.float32)  9.02 us
    all_to_all x1, starting transfers between devices, from_everyone(): return lax.all_to_all(copies, axis, split_axis=0, concat_axis=0, tiled=True)  7.22 us
    dot_general x1, matrix products, local(): jnp.dot(pool_mixed, out_pool, preferred_element_type=jnp.float32)  5.57 us
    all_gather x2, waiting for transfers between devices, sent_together(): lax.all_gather(both, axis, axis=dim, tiled=True)  5.16 us
    dot_general x1, matrix products, local(): jnp.dot(attended, out_attend, preferred_element_type=jnp.float32)  4.81 us
  transfers between devices with their start and end apart: 8, of which 3 were waited for; matrix products, arithmetic and copies ran while one was open for 20% of the time, Pallas kernels for 0%

profile of v1, /device:TPU:0, one launch (start us, length us, event | category | flops | bytes accessed | tf_op | source)
XLA Modules:
  0.0 153.3 jit_solution(9261544442912208577)
XLA Ops:
  6.5 0.8 copy.33
  7.4 0.8 copy.34
  8.2 1.5 pad_maximum_fusion.3
  9.7 0.0 all-gather.3.cloned.1.call-update
  9.7 1.2 fusion.2
  10.9 1.2 fusion.4
  12.1 2.0 %stack.2 = bf16[8,96,2048]{2,1,0:T(8,128)(2,1)} broadcast(bf16[96,2048]{1,0:T(8,128)(2,1)S(1)} %fusion.4), dimensions={1,2} | broadcast | bytes 3538944 | tf_op jit(solution)/shard_map/stack | solution.py:61
  14.1 4.7 %all-to-all-start = ((bf16[8,96,2048]{2,1,0:T(8,128)(2,1)}), bf16[8,96,2048]{2,1,0:T(8,128)(2,1)S(1)}, u32[]{:S(2)}, u32[]{:S(2)}) async-start(bf16[8,96,2048]{2,1,0:T(8,128)(2,1)} %stack.2), calls=%async_computation | async-start | bytes 6291456 | tf_op jit(solution)/shard_map/all_to_all | solution.py:61
  18.9 0.0 all-gather.5.cloned.1.call-start
  18.9 0.0 copy-done.7
  18.9 0.0 copy-done.8
  18.9 0.6 pad_maximum_fusion.4
  19.5 0.0 all-gather.5.cloned.1.call-update
  19.7 1.0 fusion.8
  20.7 36.6 %all-to-all-done = bf16[8,96,2048]{2,1,0:T(8,128)(2,1)S(1)} async-done(((bf16[8,96,2048]{2,1,0:T(8,128)(2,1)}), bf16[8,96,2048]{2,1,0:T(8,128)(2,1)S(1)}, u32[]{:S(2)}, u32[]{:S(2)}) %all-to-all-start) | async-done | bytes 3145760 | tf_op jit(solution)/shard_map/all_to_all | solution.py:61
  57.3 2.1 %convolution_convert_fusion.3 = bf16[768,64]{0,1:T(8,128)(2,1)S(1)} fusion(bf16[768,2048]{1,0:T(8,128)(2,1)S(1)} %bitcast.59, bf16[2048,384]{1,0:T(8,128)(2,1)} %all-gather.3.cloned.1.call-done), kind=kOutput, calls=%fused_computation.9 | convolution fusion | flops 201375744 | bytes 3768320 | tf_op jit(solution)/shard_map/dot_general | solution.py:66
  59.4 0.6 slice.62
  60.0 0.0 copy-done.5
  60.0 0.1 slice.53
  60.2 2.2 %convolution_convert_fusion.4 = bf16[768,64]{0,1:T(8,128)(2,1)S(1)} fusion(bf16[768,2048]{1,0:T(8,128)(2,1)S(1)} %bitcast.60, bf16[2048,384]{1,0:T(8,128)(2,1)} %all-gather.3.cloned.1.call-done), kind=kOutput, calls=%fused_computation.10 | convolution fusion | flops 201375744 | bytes 3768320 | tf_op jit(solution)/shard_map/dot_general | solution.py:66
  62.4 0.6 slice.61
  63.0 0.1 slice.49
  63.2 4.0 %collective-permute-start.1 = (bf16[128,64]{0,1:T(8,128)(2,1)}, bf16[128,64]{0,1:T(8,128)(2,1)}, u32[]{:S(2)}, u32[]{:S(2)}) collective-permute-start(bf16[128,64]{0,1:T(8,128)(2,1)} %slice.62), channel_id=1, source_target_pairs={{0,8},{8,16},{16,24},{24,32},{32,40},{40,48},{48,56},{56,64},{64,7... | collective-permute-start | bytes 49160 | tf_op jit(solution)/shard_map/ppermute | solution.py:26
  67.1 0.6 copy.38
  67.8 3.4 %collective-permute-start = (bf16[128,64]{0,1:T(8,128)(2,1)}, bf16[128,64]{0,1:T(8,128)(2,1)}, u32[]{:S(2)}, u32[]{:S(2)}) collective-permute-start(bf16[128,64]{0,1:T(8,128)(2,1)} %slice.61), channel_id=1, source_target_pairs={{0,8},{8,16},{16,24},{24,32},{32,40},{40,48},{48,56},{56,64},{64,7... | collective-permute-start | bytes 49160 | tf_op jit(solution)/shard_map/ppermute | solution.py:26
  71.2 0.0 copy-done.3
  71.2 0.6 copy.36
  71.8 2.0 %fusion.45 = (f32[768,128]{1,0:T(8,128)S(1)}, bf16[768,128]{1,0:T(8,128)(2,1)S(1)}) fusion(bf16[768,2048]{1,0:T(8,128)(2,1)S(1)} %bitcast.61, bf16[2048,384]{1,0:T(8,128)(2,1)} %all-gather.3.cloned.1.call-done), kind=kOutput, calls=%fused_computation.79 | convolution fusion | flops 402849792 | bytes 4259840 | tf_op jit(solution)/shard_map/dot_general | solution.py:66
  73.8 0.0 copy-start
  73.9 0.7 copy-done
  74.5 0.6 slice.63
  75.1 3.1 %collective-permute-start.2 = (bf16[128,128]{1,0:T(8,128)(2,1)}, bf16[128,128]{1,0:T(8,128)(2,1)}, u32[]{:S(2)}, u32[]{:S(2)}) collective-permute-start(bf16[128,128]{1,0:T(8,128)(2,1)} %slice.63), channel_id=1, source_target_pairs={{0,8},{8,16},{16,24},{24,32},{32,40},{40,48},{48,56},{56,64},{64,7... | collective-permute-start | bytes 98312 | tf_op jit(solution)/shard_map/ppermute | solution.py:26
  78.2 2.7 %convolution_convert_fusion.1 = bf16[768,128]{1,0:T(8,128)(2,1)} fusion(bf16[768,2048]{1,0:T(8,128)(2,1)S(1)} %bitcast.62, bf16[2048,384]{1,0:T(8,128)(2,1)} %all-gather.3.cloned.1.call-done), kind=kOutput, calls=%fused_computation.6 | convolution fusion | flops 402751488 | bytes 3866624 | tf_op jit(solution)/shard_map/dot_general | solution.py:66
  80.9 1.1 reshape.127
  82.0 0.0 collective-permute-done.1
  82.1 0.9 pad_maximum_fusion.1
  83.0 0.0 copy-start.9
  83.0 0.1 slice.52
  83.1 0.0 copy-start.4
  83.1 1.5 fusion.44
  84.6 0.1 broadcast_maximum_fusion
  84.7 0.2 fusion
  84.9 0.1 exponential_add_fusion
  85.0 0.0 collective-permute-done
  85.0 0.0 copy-done.4
  85.1 0.7 pad_maximum_fusion.2
  85.8 0.1 slice.48
  85.9 0.0 copy-done.6
  86.0 0.4 fusion.1
  86.4 0.1 copy.42
  86.5 0.0 collective-permute-done.2
  86.5 0.8 convert_element_type.66
  87.3 0.3 fusion.17
  87.7 0.1 copy.44
  87.8 0.6 broadcast_in_dim.40
  88.4 7.2 %all-to-all-start.1 = ((f32[16,1,128]{2,1,0:T(1,128)}), f32[16,1,128]{2,1,0:T(1,128)S(1)}, u32[]{:S(2)}, u32[]{:S(2)}) async-start(f32[16,1,128]{2,1,0:T(1,128)} %broadcast_in_dim.40), calls=%async_computation.1 | async-start | bytes 16384 | tf_op jit(solution)/shard_map/all_to_all | solution.py:31
  95.7 0.0 reduce-scatter.2.cloned.1.call-start
  95.7 5.2 %all-gather.5.cloned.1.call-done = bf16[256,2048]{1,0:T(8,128)(2,1)} async-done(((bf16[256,128]{1,0:T(8,128)(2,1)}), bf16[256,2048]{1,0:T(8,128)(2,1)}) %all-gather.5.cloned.1.call-update) | async-done | bytes 1048592 | tf_op jit(solution)/shard_map/all_gather | solution.py:20
  100.9 4.8 %fusion.12 = f32[768,2048]{1,0:T(8,128)} fusion(bf16[256,2048]{1,0:T(8,128)(2,1)} %all-gather.5.cloned.1.call-done, bf16[16,8,6,128]{3,2,1,0:T(8,128)(2,1)S(1)} %bitcast.67), kind=kOutput, calls=%fused_computation.25 | convolution fusion | flops 402653184 | bytes 7012352 | tf_op jit(solution)/shard_map/dot_general | solution.py:143
  105.7 0.0 all-to-all-done.1
  105.7 0.1 select_reduce_fusion
  105.8 5.6 %add_convert_fusion = bf16[768,2048]{1,0:T(8,128)(2,1)} fusion(f32[768,2048]{1,0:T(8,128)} %fusion.12, bf16[256,2048]{1,0:T(8,128)(2,1)S(1)} %copy-done.2, s32[]{:T(128)S(6)} %select_n.38, f32[896,128]{1,0:T(8,128)S(1)} %bitcast.65, f32[768,128]{1,0:T(8,128)S(1)} %slice_subtract_fusion, f32[128]{0:T(128)S(1)} %copy-done.10, f32[768]{0:T(1024)S(1)} %get-tuple-element.9, ...), kind=kOutput, calls=%fused_computation | convolution fusion | flops 406683648 | bytes 11412485 | tf_op jit(solution)/shard_map/dot_general | solution.py:144
  111.4 0.0 reduce-scatter.2.cloned.1.call-update
  111.4 35.3 %reduce-scatter.2.cloned.1.call-done = bf16[96,2048]{1,0:T(8,128)(2,1)} async-done(((bf16[768,2048]{1,0:T(8,128)(2,1)}), bf16[96,2048]{1,0:T(8,128)(2,1)}) %reduce-scatter.2.cloned.1.call-update) | async-done | bytes 393232 | tf_op jit(solution)/shard_map/reduce_scatter | solution.py:141
  (28 shorter events, 0.2 us)
Async XLA Ops:
  6.5 50.7 %all-gather.3.cloned.1.call-start = ((), (), s32[]{:S(2)}) async-start(), calls=%async_computation.3 | async-start | bytes 1671168 | tf_op jit(solution)/shard_map/all_gather | solution.py:20
  14.1 4.8 %copy-start.7 = (bf16[128,128]{1,0:T(8,128)(2,1)S(1)}, bf16[128,128]{1,0:T(8,128)(2,1)}, u32[]{:S(2)}) copy-start(bf16[128,128]{1,0:T(8,128)(2,1)} %param.19) | copy-start | bytes 98308
  14.1 4.8 %copy-start.8 = (bf16[128,128]{1,0:T(8,128)(2,1)S(1)}, bf16[128,128]{1,0:T(8,128)(2,1)}, u32[]{:S(2)}) copy-start(bf16[128,128]{1,0:T(8,128)(2,1)} %param.18) | copy-start | bytes 98308
  14.1 43.1 %all-to-all-start = ((bf16[8,96,2048]{2,1,0:T(8,128)(2,1)}), bf16[8,96,2048]{2,1,0:T(8,128)(2,1)S(1)}, u32[]{:S(2)}, u32[]{:S(2)}) async-start(bf16[8,96,2048]{2,1,0:T(8,128)(2,1)} %stack.2), calls=%async_computation | async-start | bytes 6291456 | tf_op jit(solution)/shard_map/all_to_all | solution.py:61
  18.9 82.0 %all-gather.5.cloned.1.call-start = ((), (), s32[]{:S(2)}) async-start(), calls=%async_computation.4 | async-start | bytes 1114112 | tf_op jit(solution)/shard_map/all_gather | solution.py:20
  59.4 0.7 copy-start.5
  62.4 8.8 %copy-start.3 = (bf16[768,64]{0,1:T(8,128)(2,1)}, bf16[768,64]{0,1:T(8,128)(2,1)S(1)}, u32[]{:S(2)}) copy-start(bf16[768,64]{0,1:T(8,128)(2,1)S(1)} %convolution_convert_fusion.4) | copy-start | bytes 294916
  63.2 18.9 %collective-permute-start.1 = (bf16[128,64]{0,1:T(8,128)(2,1)}, bf16[128,64]{0,1:T(8,128)(2,1)}, u32[]{:S(2)}, u32[]{:S(2)}) collective-permute-start(bf16[128,64]{0,1:T(8,128)(2,1)} %slice.62), channel_id=1, source_target_pairs={{0,8},{8,16},{16,24},{24,32},{32,40},{40,48},{48,56},{56,64},{64,7... | collective-permute-start | bytes 49160 | tf_op jit(solution)/shard_map/ppermute | solution.py:26
  67.8 17.2 %collective-permute-start = (bf16[128,64]{0,1:T(8,128)(2,1)}, bf16[128,64]{0,1:T(8,128)(2,1)}, u32[]{:S(2)}, u32[]{:S(2)}) collective-permute-start(bf16[128,64]{0,1:T(8,128)(2,1)} %slice.61), channel_id=1, source_target_pairs={{0,8},{8,16},{16,24},{24,32},{32,40},{40,48},{48,56},{56,64},{64,7... | collective-permute-start | bytes 49160 | tf_op jit(solution)/shard_map/ppermute | solution.py:26
  73.8 0.7 copy-start
  75.1 11.4 %collective-permute-start.2 = (bf16[128,128]{1,0:T(8,128)(2,1)}, bf16[128,128]{1,0:T(8,128)(2,1)}, u32[]{:S(2)}, u32[]{:S(2)}) collective-permute-start(bf16[128,128]{1,0:T(8,128)(2,1)} %slice.63), channel_id=1, source_target_pairs={{0,8},{8,16},{16,24},{24,32},{32,40},{40,48},{48,56},{56,64},{64,7... | collective-permute-start | bytes 98312 | tf_op jit(solution)/shard_map/ppermute | solution.py:26
  83.0 1.7 %copy-start.9 = (f32[2]{0:T(128)S(1)}, f32[2]{0:T(128)}, u32[]{:S(2)}) copy-start(f32[2]{0:T(128)} %param.16) | copy-start | bytes 28
  83.1 1.9 %copy-start.4 = (bf16[768,64]{0,1:T(8,128)(2,1)S(1)}, bf16[768,64]{0,1:T(8,128)(2,1)}, u32[]{:S(2)}) copy-start(bf16[768,64]{0,1:T(8,128)(2,1)} %copy-done.3) | copy-start | bytes 294916
  84.6 1.3 copy-start.6
  88.4 17.3 %all-to-all-start.1 = ((f32[16,1,128]{2,1,0:T(1,128)}), f32[16,1,128]{2,1,0:T(1,128)S(1)}, u32[]{:S(2)}, u32[]{:S(2)}) async-start(f32[16,1,128]{2,1,0:T(1,128)} %broadcast_in_dim.40), calls=%async_computation.1 | async-start | bytes 16384 | tf_op jit(solution)/shard_map/all_to_all | solution.py:31
  95.7 51.1 %reduce-scatter.2.cloned.1.call-start = ((), (), s32[]{:S(2)}) async-start(), calls=%async_computation.5 | async-start | bytes 3538944 | tf_op jit(solution)/shard_map/reduce_scatter | solution.py:141
  100.9 4.9 %copy-start.1 = (bf16[768,128]{1,0:T(8,128)(2,1)S(1)}, bf16[768,128]{1,0:T(8,128)(2,1)}, u32[]{:S(2)}) copy-start(bf16[768,128]{1,0:T(8,128)(2,1)} %copy-done) | copy-start | bytes 589828
  100.9 4.9 %copy-start.2 = (bf16[256,2048]{1,0:T(8,128)(2,1)S(1)}, bf16[256,2048]{1,0:T(8,128)(2,1)}, u32[]{:S(2)}) copy-start(bf16[256,2048]{1,0:T(8,128)(2,1)} %all-gather.5.cloned.1.call-done) | copy-start | bytes 3145732
  100.9 4.9 %copy-start.10 = (f32[128]{0:T(128)S(1)}, f32[128]{0:T(128)}, u32[]{:S(2)}) copy-start(f32[128]{0:T(128)} %param.17) | copy-start | bytes 1540
Sparse Core Ops, SparseCore 0:
  9.9 46.2 all-gather.2
  58.3 42.5 all-gather.4
  111.5 35.1 reduce-scatter.1
